TPU v7x, 32 devices: a whole 2x2x4 slice. The times are simulated.
32 devices in a mesh: sp: 8 (over z, x), tp: 4 (over y, core).
Axes of the slice: x: 2, y: 2, z: 4, core: 2. Of those that a mesh axis runs over, the one named last changes fastest.
Arguments:
- pool_input: bfloat16 [2048, 256], P('sp', 'tp'), may hold values from -6 to 6
- pool_weight: bfloat16 [4, 64, 64], P('tp'), may hold values from -0.75 to 0.75
- pool_gain: bfloat16 [256], P('tp'), may hold values from 0.099609375 to 1.8984375
- out_weight: bfloat16 [256, 2048], P(None, 'tp'), may hold values from -0.375 to 0.375
- resid: bfloat16 [2048, 2048], P('sp', 'tp'), may hold values from -90 to 90
- norm_gain: bfloat16 [2048], P('tp'), may hold values from 0.099609375 to 1.8984375
- routes: int32 [2048, 2], P('sp'), may hold values from 0 to 7, all different within a row; in each aligned block of 256 rows (0 to 255, 256 to 511, ...) at most 128 rows name the same one
- route_weight: float32 [2048, 2], P('sp'), may hold values from 0.2 to 1
- expert_gate: bfloat16 [8, 2048, 4096], P('sp', None, 'tp'), may hold values from -0.375 to 0.375
- expert_up: bfloat16 [8, 2048, 4096], P('sp', None, 'tp'), may hold values from -0.375 to 0.375
- expert_down: bfloat16 [8, 4096, 2048], P('sp', 'tp'), may hold values from -0.0234375 to 0.0234375
Outputs:
- layer_out: bfloat16 [2048, 2048], P('sp', 'tp')
Inputs may be any that keep to these rules, and one draw needn't show every extreme that they name: `routes`: the 2 experts of a position differ. In each aligned block of 256 positions no expert is named by more than 128 assignments; some block reaches that bound.
All inputs are finite; a program needn't handle non-finite values.
Results may differ from a plain program's by a relative error of at most 0.0085.
Values may be sent and summed in bfloat16 or wider, within the bound.
A program may use at most 64 MiB of HBM per device.

v0:
```python
import jax
import jax.numpy as jnp
from jax import lax
from jax.sharding import PartitionSpec as P

D = 2048
GSIZE = 64
REACH = 16
TOPK = 2
GATE_LIMIT = 7.0
GATE_ALPHA = 1.702
NORM_EPS = 1e-05


def from_behind(value, axis, steps):
    count = lax.axis_size(axis)
    first, last = (max(0, -steps), min(count, count - steps))
    return lax.ppermute(value, axis, [(source, source + steps) for source in range(first, last)])


def clamped_unit(gate_pre, up_pre):
    gate_cut = jnp.minimum(gate_pre, GATE_LIMIT)
    up_cut = jnp.clip(up_pre, -GATE_LIMIT, GATE_LIMIT)
    return (up_cut + 1.0) * gate_cut * jax.nn.sigmoid(GATE_ALPHA * gate_cut)


def window_pool(extended, width_of, position, tok_count):
    summed = jnp.zeros((tok_count, extended.shape[1]), jnp.float32)
    for offset in range(REACH):
        first_row = REACH - 1 - offset
        shifted = extended[first_row : first_row + tok_count]
        summed = summed + jnp.where(offset < width_of[None, :], shifted, 0.0)
    counted = jnp.minimum(position[:, None] + 1, width_of[None, :]).astype(jnp.float32)
    current = extended[REACH - 1 :]
    return (summed / counted - current).astype(jnp.bfloat16)


def slot_of(route_block, expert_count, capacity):
    flattened = route_block.reshape(-1)
    onehot = (flattened[:, None] == jnp.arange(expert_count, dtype=jnp.int32)[None, :]).astype(
        jnp.int32
    )
    earlier = jnp.cumsum(onehot, axis=0) - onehot
    ranked = jnp.sum(earlier * onehot, axis=1)
    return flattened * capacity + ranked


def on_device(
    pool_input,
    pool_weight,
    pool_gain,
    out_weight,
    resid,
    norm_gain,
    routes,
    route_weight,
    expert_gate,
    expert_up,
    expert_down,
):
    tok_rows, channels = pool_input.shape
    groups = pool_weight.shape[0]
    features = out_weight.shape[1]
    experts_all = lax.axis_size("sp") * expert_gate.shape[0]
    capacity = 2 * tok_rows * TOPK // experts_all
    tail_rows = pool_input[tok_rows - (REACH - 1) :]
    before = from_behind(tail_rows, "sp", 1)
    extended = jnp.concatenate([before, pool_input], axis=0).astype(jnp.float32)
    first_group = lax.axis_index("tp") * groups
    width_of = 2 ** (1 + (first_group + jnp.arange(channels, dtype=jnp.int32) // GSIZE) % 4)
    position = lax.axis_index("sp") * tok_rows + jnp.arange(tok_rows, dtype=jnp.int32)
    pooled = window_pool(extended, width_of, position, tok_rows)
    grouped = jnp.einsum(
        "tgc,gcd->tgd",
        pooled.reshape(tok_rows, groups, GSIZE),
        pool_weight,
        preferred_element_type=jnp.float32,
    )
    mixed_out = (
        (grouped * pool_gain.astype(jnp.float32).reshape(groups, GSIZE))
        .astype(jnp.bfloat16)
        .reshape(tok_rows, channels)
    )
    projected = jnp.dot(
        lax.all_gather(mixed_out, "tp", axis=1, tiled=True),
        out_weight,
        preferred_element_type=jnp.float32,
    )
    stored = lax.optimization_barrier((resid.astype(jnp.float32) + projected).astype(jnp.bfloat16))
    stream = stored.astype(jnp.float32)
    squares = lax.psum(jnp.sum(stream * stream, axis=1), "tp")
    scale_row = lax.rsqrt(squares / D + NORM_EPS)
    normed_part = (stream * scale_row[:, None] * norm_gain.astype(jnp.float32)).astype(jnp.bfloat16)
    slot_index = slot_of(routes, experts_all, capacity)
    token_ids = jnp.repeat(jnp.arange(tok_rows, dtype=jnp.int32), TOPK)
    slot_token = (
        jnp.full((experts_all * capacity,), tok_rows, jnp.int32).at[slot_index].set(token_ids)
    )
    sent_rows = jnp.take(normed_part, slot_token, axis=0, mode="fill", fill_value=0).reshape(
        experts_all, capacity, features
    )
    gathered = lax.all_gather(
        lax.all_to_all(sent_rows, "sp", split_axis=0, concat_axis=0, tiled=True),
        "tp",
        axis=2,
        tiled=True,
    )
    sources = gathered.shape[0]
    slot_count = gathered.shape[1]
    flattened = gathered.reshape(sources * slot_count, gathered.shape[2])
    gate_pre = jnp.dot(flattened, expert_gate[0], preferred_element_type=jnp.float32)
    up_pre = jnp.dot(flattened, expert_up[0], preferred_element_type=jnp.float32)
    hidden = clamped_unit(gate_pre, up_pre).astype(jnp.bfloat16)
    down_piece = expert_down[0]
    summed = lax.psum_scatter(
        lax.dot_general(
            down_piece, hidden, (((0,), (1,)), ((), ())), preferred_element_type=jnp.float32
        ).astype(jnp.bfloat16),
        "tp",
        scatter_dimension=0,
        tiled=True,
    ).astype(jnp.float32)
    result = summed.astype(jnp.bfloat16).reshape(summed.shape[0], sources, slot_count)
    returned = lax.all_to_all(result, "sp", split_axis=1, concat_axis=1, tiled=True)
    flat_back = returned.reshape(returned.shape[0], experts_all * capacity)
    picked = (
        jnp.take(flat_back, slot_index, axis=1)
        .astype(jnp.float32)
        .reshape(flat_back.shape[0], tok_rows, TOPK)
    )
    combined = jnp.sum(picked * route_weight[None, :, :], axis=2)
    return (stream + combined.T).astype(jnp.bfloat16)


def solution(mesh):
    in_specs = (
        P("sp", "tp"),
        P("tp", None, None),
        P("tp"),
        P(None, "tp"),
        P("sp", "tp"),
        P("tp"),
        P("sp", None),
        P("sp", None),
        P("sp", None, "tp"),
        P("sp", None, "tp"),
        P("sp", "tp", None),
    )
    out_specs = P("sp", "tp")
    return jax.shard_map(
        on_device, mesh=mesh, in_specs=in_specs, out_specs=out_specs, check_vma=False
    )
```

profile of v0, /device:TPU:0, one launch (start us, length us, event | category | flops | bytes accessed | tf_op | source)
XLA Modules:
  0.0 210.5 jit_solution(373483035602310403)
XLA Ops:
  6.5 0.0 copy-start
  6.5 0.0 all-gather.3.cloned.1.call-start
  6.5 0.8 slice.58
  7.4 4.9 %collective-permute-start = (bf16[15,64]{0,1:T(8,128)(2,1)S(1)}, bf16[15,64]{0,1:T(8,128)(2,1)S(1)}, u32[]{:S(2)}, u32[]{:S(2)}) collective-permute-start(bf16[15,64]{0,1:T(8,128)(2,1)S(1)} %slice.58), channel_id=1, source_target_pairs={{0,4},{4,8},{8,12},{12,16},{16,20},{20,24},{24,28},{1,5},{5,9},{9,... | collective-permute-start | bytes 5768 | tf_op jit(solution)/shard_map/ppermute | solution.py:18
  12.5 0.8 copy.18
  13.3 0.1 eq.28
  13.4 0.1 reshape.227
  13.6 0.7 broadcast_multiply_fusion
  14.3 1.1 reduce-window.6
  15.4 0.2 slice_reduce_fusion
  15.6 0.1 copy.22
  15.8 0.1 mul.320
  16.0 0.1 reshape.253
  16.1 0.1 fusion.39
  16.2 2.4 %scatter_custom_fusion = s32[1024]{0:T(1024)S(1)} fusion(s32[512]{0:T(512)S(1)} %bitcast.63, s32[512]{0:T(512)S(1)} %reshape.253, s32[]{:T(128)} %constant.149.clone.1), kind=kCustom, calls=%fused_computation.79 | custom fusion | bytes 4100 | tf_op jit(solution)/shard_map/scatter | solution.py:97
  18.7 0.7 convert_element_type.62
  19.4 0.7 convert_element_type.69
  20.1 0.0 collective-permute-done
  20.1 0.8 maximum_convert_fusion
  20.9 1.3 fusion.13
  22.2 5.4 %all-gather = bf16[256,1,256]{0,2,1:T(8,128)(2,1)S(1)} all-gather(bf16[256,1,64]{0,2,1:T(8,128)(2,1)S(1)} %fusion.13), channel_id=2, replica_groups=mesh['sp'=8,'tp'=4] {'tp'}, dimensions={2}, use_global_device_ids=true | all-gather | bytes 163840 | tf_op jit(solution)/shard_map/all_gather | solution.py:85
  27.7 0.0 copy-done
  27.7 1.2 fusion.10
  28.9 0.1 fusion.14
  29.0 7.1 %psum.7 = f32[256]{0:T(256)S(1)} all-reduce(f32[256]{0:T(256)S(1)} %fusion.14), channel_id=1, replica_groups=mesh['sp'=8,'tp'=4] {'tp'}, use_global_device_ids=true, to_apply=%region_5.6 | all-reduce | flops 256 | bytes 2048 | tf_op jit(solution)/shard_map/psum | solution.py:91
  36.1 0.1 fusion.16
  36.3 4.0 %gather_fusion = bf16[1024,512]{1,0:T(8,128)(2,1)S(1)} fusion(bf16[256,512]{1,0:T(8,128)(2,1)S(1)} %fusion.16, s32[1024]{0:T(1024)S(1)} %fusion.42), kind=kCustom, calls=%fused_computation | custom fusion | bytes 2101248 | tf_op jit(solution)/shard_map/jit(_take)/gather | solution.py:99
  40.2 0.2 broadcast_select_fusion
  40.5 29.1 %all_to_all.10 = bf16[8,128,512]{2,1,0:T(8,128)(2,1)} all-to-all(bf16[8,128,512]{2,1,0:T(8,128)(2,1)S(1)} %broadcast_select_fusion), channel_id=1, replica_groups=mesh['sp'=8,'tp'=4] {'sp'}, dimensions={0} | all-to-all | bytes 2097152 | tf_op jit(solution)/shard_map/all_to_all | solution.py:103
  69.6 0.0 all-gather.3.cloned.1.call-update
  69.6 0.0 reduce-scatter.2.cloned.1.call-start
  69.7 33.6 %all-gather.3.cloned.1.call-done = bf16[8,128,2048]{2,1,0:T(8,128)(2,1)} async-done(((bf16[8,128,512]{2,1,0:T(8,128)(2,1)}), bf16[8,128,2048]{2,1,0:T(8,128)(2,1)}) %all-gather.3.cloned.1.call-update) | async-done | bytes 4194320 | tf_op jit(solution)/shard_map/all_gather | solution.py:102
  103.3 0.0 copy-start.3
  103.3 0.0 copy-start.5
  103.3 7.6 %fusion.2 = f32[1024,1024]{1,0:T(8,128)S(1)} fusion(bf16[1024,2048]{1,0:T(8,128)(2,1)} %bitcast.65, bf16[1,2048,1024]{2,1,0:T(8,128)(2,1)} %param.19), kind=kOutput, calls=%fused_computation.5 | convolution fusion | flops 4294967296 | bytes 12582912 | tf_op jit(solution)/shard_map/dot_general | solution.py:111
  110.9 0.0 copy-done.3
  110.9 0.0 copy-done.5
  110.9 0.0 copy-start.4
  110.9 5.7 %multiply_convert_fusion = bf16[1024,1024]{1,0:T(8,128)(2,1)S(1)} fusion(f32[1024,1024]{1,0:T(8,128)S(1)} %fusion.2, bf16[1024,2048]{1,0:T(8,128)(2,1)S(1)} %bitcast.66, bf16[1,2048,1024]{2,1,0:T(8,128)(2,1)S(1)} %copy-done.3), kind=kOutput, calls=%fused_computation.10 | convolution fusion | flops 4305453056 | bytes 14680064 | tf_op jit(solution)/shard_map/dot_general | solution.py:112
  116.6 0.0 copy-done.4
  116.6 6.1 %convert_bitcast_fusion = bf16[2048,1024]{0,1:T(8,128)(2,1)} fusion(bf16[1024,1024]{1,0:T(8,128)(2,1)S(1)} %multiply_convert_fusion, bf16[1,1024,2048]{2,1,0:T(8,128)(2,1)S(1)} %copy-done.4), kind=kOutput, calls=%fused_computation.9 | convolution fusion | flops 4297064448 | bytes 10485760 | tf_op jit(solution)/shard_map/dot_general | solution.py:116
  122.7 0.0 copy-start.1
  122.7 0.0 copy-start.2
  122.7 0.0 reduce-scatter.2.cloned.1.call-update
  122.7 44.6 %reduce-scatter.2.cloned.1.call-done = bf16[512,1024]{0,1:T(8,128)(2,1)} async-done(((bf16[2048,1024]{0,1:T(8,128)(2,1)}), bf16[512,1024]{0,1:T(8,128)(2,1)}) %reduce-scatter.2.cloned.1.call-update) | async-done | bytes 1048592 | tf_op jit(solution)/shard_map/reduce_scatter | solution.py:115
  167.3 5.5 %all-to-all-start.1 = ((bf16[512,8,128]{0,2,1:T(8,128)(2,1)}), bf16[512,8,128]{0,2,1:T(8,128)(2,1)S(1)}, u32[]{:S(2)}, u32[]{:S(2)}) async-start(bf16[512,8,128]{0,2,1:T(8,128)(2,1)} %bitcast.61), calls=%async_computation.2 | async-start | bytes 2097152 | tf_op jit(solution)/shard_map/all_to_all | solution.py:124
  172.8 0.1 reduce_sum.32
  172.9 0.1 copy.20
  173.0 0.0 copy-done.1
  173.0 0.2 copy.21
  173.2 0.0 copy-done.2
  173.2 0.1 copy.23
  173.4 25.1 %all-to-all-done.1 = bf16[512,8,128]{0,2,1:T(8,128)(2,1)S(1)} async-done(((bf16[512,8,128]{0,2,1:T(8,128)(2,1)}), bf16[512,8,128]{0,2,1:T(8,128)(2,1)S(1)}, u32[]{:S(2)}, u32[]{:S(2)}) %all-to-all-start.1) | async-done | bytes 1048608 | tf_op jit(solution)/shard_map/all_to_all | solution.py:124
  198.5 2.0 gather_fusion.1
  200.4 0.2 gather.15
  200.6 2.2 %multiply_reduce_fusion = f32[512,256]{0,1:T(8,128)S(1)} fusion(bf16[512,256,2]{0,2,1:T(2,128)(2,1)S(1)} %gather.15, pred[256,2]{1,0:T(8,128)(4,1)S(1)} %copy.21, f32[256,2]{1,0:T(8,128)S(1)} %copy.23), kind=kLoop, calls=%fused_computation.17 | loop fusion | flops 917504 | bytes 1051136 | tf_op jit(solution)/shard_map/reduce_sum | solution.py:131
  202.9 0.8 fusion.17
  (20 shorter events, 0.3 us)
Async XLA Ops:
  6.5 21.1 %copy-start = (bf16[256,512]{1,0:T(8,128)(2,1)S(1)}, bf16[256,512]{1,0:T(8,128)(2,1)}, u32[]{:S(2)}) copy-start(bf16[256,512]{1,0:T(8,128)(2,1)} %param.14) | copy-start | bytes 786436
  6.5 96.7 %all-gather.3.cloned.1.call-start = ((), (), s32[]{:S(2)}) async-start(), calls=%async_computation.3 | async-start | bytes 5242880 | tf_op jit(solution)/shard_map/all_gather | solution.py:102
  7.4 12.7 %collective-permute-start = (bf16[15,64]{0,1:T(8,128)(2,1)S(1)}, bf16[15,64]{0,1:T(8,128)(2,1)S(1)}, u32[]{:S(2)}, u32[]{:S(2)}) collective-permute-start(bf16[15,64]{0,1:T(8,128)(2,1)S(1)} %slice.58), channel_id=1, source_target_pairs={{0,4},{4,8},{8,12},{12,16},{16,20},{20,24},{24,28},{1,5},{5,9},{9,... | collective-permute-start | bytes 5768 | tf_op jit(solution)/shard_map/ppermute | solution.py:18
  69.6 97.7 %reduce-scatter.2.cloned.1.call-start = ((), (), s32[]{:S(2)}) async-start(), calls=%async_computation.4 | async-start | bytes 5242880 | tf_op jit(solution)/shard_map/reduce_scatter | solution.py:115
  103.3 7.7 %copy-start.3 = (bf16[1,2048,1024]{2,1,0:T(8,128)(2,1)S(1)}, bf16[1,2048,1024]{2,1,0:T(8,128)(2,1)}, u32[]{:S(2)}) copy-start(bf16[1,2048,1024]{2,1,0:T(8,128)(2,1)} %param.20) | copy-start | bytes 12582916
  103.3 7.7 %copy-start.5 = (bf16[8,128,2048]{2,1,0:T(8,128)(2,1)S(1)}, bf16[8,128,2048]{2,1,0:T(8,128)(2,1)}, u32[]{:S(2)}) copy-start(bf16[8,128,2048]{2,1,0:T(8,128)(2,1)} %all-gather.3.cloned.1.call-done) | copy-start | bytes 12582916
  110.9 5.7 %copy-start.4 = (bf16[1,1024,2048]{2,1,0:T(8,128)(2,1)S(1)}, bf16[1,1024,2048]{2,1,0:T(8,128)(2,1)}, u32[]{:S(2)}) copy-start(bf16[1,1024,2048]{2,1,0:T(8,128)(2,1)} %param.21) | copy-start | bytes 12582916
  122.7 50.3 %copy-start.1 = (s32[256,2]{0,1:T(2,128)S(1)}, s32[256,2]{0,1:T(2,128)}, u32[]{:S(2)}) copy-start(s32[256,2]{0,1:T(2,128)} %param.17) | copy-start | bytes 6148
  122.7 50.5 %copy-start.2 = (f32[256,2]{0,1:T(2,128)S(1)}, f32[256,2]{0,1:T(2,128)}, u32[]{:S(2)}) copy-start(f32[256,2]{0,1:T(2,128)} %param.18) | copy-start | bytes 6148
  167.3 31.2 %all-to-all-start.1 = ((bf16[512,8,128]{0,2,1:T(8,128)(2,1)}), bf16[512,8,128]{0,2,1:T(8,128)(2,1)S(1)}, u32[]{:S(2)}, u32[]{:S(2)}) async-start(bf16[512,8,128]{0,2,1:T(8,128)(2,1)} %bitcast.61), calls=%async_computation.2 | async-start | bytes 2097152 | tf_op jit(solution)/shard_map/all_to_all | solution.py:124
Sparse Core Ops, SparseCore 0:
  69.7 33.4 all-gather.2
  122.8 44.3 reduce-scatter.1
where the time goes:
time: 211 us; the launch traced here: 210 us
  waiting for transfers between devices  103 us (49%)
  blocking collectives  41.7 us (20%)
  matrix products  21.9 us (10%)
  between operations  13.7 us (6%)
  local copies, waits for them, and re-layouts  11.7 us (6%)
  starting transfers between devices  10.4 us (5%)
  other arithmetic  7.86 us (4%)
    reduce_scatter x1, waiting for transfers between devices, on_device(): lax.psum_scatter(lax.dot_general(down_piece, hidden, (((0,), (1,)), ((),...  44.6 us
    all_gather x1, waiting for transfers between devices, on_device(): lax.all_gather(lax.all_to_all(sent_rows, 'sp', split_axis=0, concat_axis=...  33.6 us
    all_to_all x1, blocking collectives, on_device(): lax.all_to_all(sent_rows, 'sp', split_axis=0, concat_axis=0, tiled=True)  29.1 us
    all_to_all x1, waiting for transfers between devices, on_device(): lax.all_to_all(result, 'sp', split_axis=1, concat_axis=1, tiled=True)  25.1 us
    dot_general x1, matrix products, on_device(): jnp.dot(flattened, expert_gate[0], preferred_element_type=jnp.float32)  7.64 us
    psum x1, blocking collectives, on_device(): squares = lax.psum(jnp.sum(stream * stream, axis=1), 'tp')  7.13 us
    dot_general x1, matrix products, on_device(): lax.dot_general(down_piece, hidden, (((0,), (1,)), ((), ())), preferred_e...  6.07 us
    dot_general x1, matrix products, on_device(): jnp.dot(flattened, expert_up[0], preferred_element_type=jnp.float32)  5.66 us
  transfers between devices with their start and end apart: 4, of which 3 were waited for; matrix products, arithmetic and copies ran while one was open for 4% of the time, Pallas kernels for 0%

commit v1 on v0

--- a/solution.py
+++ b/solution.py
@@ -121,7 +121,9 @@
         tiled=True,
     ).astype(jnp.float32)
     result = summed.astype(jnp.bfloat16).reshape(summed.shape[0], sources, slot_count)
-    returned = lax.all_to_all(result, "sp", split_axis=1, concat_axis=1, tiled=True)
+    cells = jnp.split(result, lax.axis_size("sp"), axis=1)
+    got = lax.all_to_all(jnp.stack(cells), "sp", 0, 0)
+    returned = jnp.concatenate(got, axis=1)
     flat_back = returned.reshape(returned.shape[0], experts_all * capacity)
     picked = (
         jnp.take(flat_back, slot_index, axis=1)

time: 211 us -> 224 us (1.062)
  local copies, waits for them, and re-layouts: 11.7 us -> 24.2 us
    unnamed x14 -> x21, local copies, waits for them, and re-layouts: 0.97 us -> 11.9 us
where the time goes in v1:
time: 224 us; the launch traced here: 223 us
  waiting for transfers between devices  103 us (46%)
  blocking collectives  41.7 us (19%)
  local copies, waits for them, and re-layouts  24.2 us (11%)
  matrix products  21.9 us (10%)
  between operations  13.7 us (6%)
  starting transfers between devices  10.4 us (5%)
  other arithmetic  7.86 us (4%)
    reduce_scatter x1, waiting for transfers between devices, on_device(): lax.psum_scatter(lax.dot_general(down_piece, hidden, (((0,), (1,)), ((),...  44.6 us
    all_gather x1, waiting for transfers between devices, on_device(): lax.all_gather(lax.all_to_all(sent_rows, 'sp', split_axis=0, concat_axis=...  33.6 us
    all_to_all x1, blocking collectives, on_device(): lax.all_to_all(sent_rows, 'sp', split_axis=0, concat_axis=0, tiled=True)  29.1 us
    all_to_all x1, waiting for transfers between devices, on_device(): got = lax.all_to_all(jnp.stack(cells), 'sp', 0, 0)  25.1 us
    unnamed x21, local copies, waits for them, and re-layouts  11.9 us
    dot_general x1, matrix products, on_device(): jnp.dot(flattened, expert_gate[0], preferred_element_type=jnp.float32)  7.64 us
    psum x1, blocking collectives, on_device(): squares = lax.psum(jnp.sum(stream * stream, axis=1), 'tp')  7.13 us
    dot_general x1, matrix products, on_device(): lax.dot_general(down_piece, hidden, (((0,), (1,)), ((), ())), preferred_e...  6.07 us
  transfers between devices with their start and end apart: 4, of which 3 were waited for; matrix products, arithmetic and copies ran while one was open for 4% of the time, Pallas kernels for 0%

profile of v1, /device:TPU:0, one launch (start us, length us, event | category | flops | bytes accessed | tf_op | source)
XLA Modules:
  0.0 223.0 jit_solution(5382660900606504322)
XLA Ops:
  6.5 0.0 copy-start
  6.5 0.0 all-gather.3.cloned.1.call-start
  6.5 0.8 slice.58
  7.4 4.9 %collective-permute-start = (bf16[15,64]{0,1:T(8,128)(2,1)S(1)}, bf16[15,64]{0,1:T(8,128)(2,1)S(1)}, u32[]{:S(2)}, u32[]{:S(2)}) collective-permute-start(bf16[15,64]{0,1:T(8,128)(2,1)S(1)} %slice.58), channel_id=1, source_target_pairs={{0,4},{4,8},{8,12},{12,16},{16,20},{20,24},{24,28},{1,5},{5,9},{9,... | collective-permute-start | bytes 5768 | tf_op jit(solution)/shard_map/ppermute | solution.py:18
  12.5 0.8 copy.18
  13.3 0.1 eq.28
  13.4 0.1 reshape.227
  13.6 0.7 broadcast_multiply_fusion
  14.3 1.1 reduce-window.6
  15.4 0.2 slice_reduce_fusion
  15.6 0.1 copy.22
  15.8 0.1 mul.320
  16.0 0.1 reshape.253
  16.1 0.1 fusion.47
  16.2 2.4 %scatter_custom_fusion = s32[1024]{0:T(1024)S(1)} fusion(s32[512]{0:T(512)S(1)} %bitcast.104, s32[512]{0:T(512)S(1)} %reshape.253, s32[]{:T(128)} %constant.149.clone.1), kind=kCustom, calls=%fused_computation.95 | custom fusion | bytes 4100 | tf_op jit(solution)/shard_map/scatter | solution.py:97
  18.7 0.7 convert_element_type.62
  19.4 0.7 convert_element_type.69
  20.1 0.0 collective-permute-done
  20.1 0.8 maximum_convert_fusion
  20.9 1.3 fusion.13
  22.2 5.4 %all-gather = bf16[256,1,256]{0,2,1:T(8,128)(2,1)S(1)} all-gather(bf16[256,1,64]{0,2,1:T(8,128)(2,1)S(1)} %fusion.13), channel_id=2, replica_groups=mesh['sp'=8,'tp'=4] {'tp'}, dimensions={2}, use_global_device_ids=true | all-gather | bytes 163840 | tf_op jit(solution)/shard_map/all_gather | solution.py:85
  27.7 0.0 copy-done
  27.7 1.2 fusion.10
  28.9 0.1 fusion.14
  29.0 7.1 %psum.7 = f32[256]{0:T(256)S(1)} all-reduce(f32[256]{0:T(256)S(1)} %fusion.14), channel_id=1, replica_groups=mesh['sp'=8,'tp'=4] {'tp'}, use_global_device_ids=true, to_apply=%region_5.6 | all-reduce | flops 256 | bytes 2048 | tf_op jit(solution)/shard_map/psum | solution.py:91
  36.1 0.1 fusion.16
  36.3 4.0 %gather_fusion = bf16[1024,512]{1,0:T(8,128)(2,1)S(1)} fusion(bf16[256,512]{1,0:T(8,128)(2,1)S(1)} %fusion.16, s32[1024]{0:T(1024)S(1)} %fusion.50), kind=kCustom, calls=%fused_computation | custom fusion | bytes 2101248 | tf_op jit(solution)/shard_map/jit(_take)/gather | solution.py:99
  40.2 0.2 broadcast_select_fusion
  40.5 29.1 %all_to_all.10 = bf16[8,128,512]{2,1,0:T(8,128)(2,1)} all-to-all(bf16[8,128,512]{2,1,0:T(8,128)(2,1)S(1)} %broadcast_select_fusion), channel_id=1, replica_groups=mesh['sp'=8,'tp'=4] {'sp'}, dimensions={0} | all-to-all | bytes 2097152 | tf_op jit(solution)/shard_map/all_to_all | solution.py:103
  69.6 0.0 all-gather.3.cloned.1.call-update
  69.6 0.0 reduce-scatter.2.cloned.1.call-start
  69.7 33.6 %all-gather.3.cloned.1.call-done = bf16[8,128,2048]{2,1,0:T(8,128)(2,1)} async-done(((bf16[8,128,512]{2,1,0:T(8,128)(2,1)}), bf16[8,128,2048]{2,1,0:T(8,128)(2,1)}) %all-gather.3.cloned.1.call-update) | async-done | bytes 4194320 | tf_op jit(solution)/shard_map/all_gather | solution.py:102
  103.3 0.0 copy-start.3
  103.3 0.0 copy-start.5
  103.3 7.6 %fusion.2 = f32[1024,1024]{1,0:T(8,128)S(1)} fusion(bf16[1024,2048]{1,0:T(8,128)(2,1)} %bitcast.106, bf16[1,2048,1024]{2,1,0:T(8,128)(2,1)} %param.19), kind=kOutput, calls=%fused_computation.5 | convolution fusion | flops 4294967296 | bytes 12582912 | tf_op jit(solution)/shard_map/dot_general | solution.py:111
  110.9 0.0 copy-done.3
  110.9 0.0 copy-done.5
  110.9 0.0 copy-start.4
  110.9 5.7 %multiply_convert_fusion = bf16[1024,1024]{1,0:T(8,128)(2,1)S(1)} fusion(f32[1024,1024]{1,0:T(8,128)S(1)} %fusion.2, bf16[1024,2048]{1,0:T(8,128)(2,1)S(1)} %bitcast.107, bf16[1,2048,1024]{2,1,0:T(8,128)(2,1)S(1)} %copy-done.3), kind=kOutput, calls=%fused_computation.10 | convolution fusion | flops 4305453056 | bytes 14680064 | tf_op jit(solution)/shard_map/dot_general | solution.py:112
  116.6 0.0 copy-done.4
  116.6 6.1 %convert_bitcast_fusion = bf16[2048,1024]{0,1:T(8,128)(2,1)} fusion(bf16[1024,1024]{1,0:T(8,128)(2,1)S(1)} %multiply_convert_fusion, bf16[1,1024,2048]{2,1,0:T(8,128)(2,1)S(1)} %copy-done.4), kind=kOutput, calls=%fused_computation.9 | convolution fusion | flops 4297064448 | bytes 10485760 | tf_op jit(solution)/shard_map/dot_general | solution.py:116
  122.7 0.0 copy-start.1
  122.7 0.0 reduce-scatter.2.cloned.1.call-update
  122.7 44.6 %reduce-scatter.2.cloned.1.call-done = bf16[512,1024]{0,1:T(8,128)(2,1)} async-done(((bf16[2048,1024]{0,1:T(8,128)(2,1)}), bf16[512,1024]{0,1:T(8,128)(2,1)}) %reduce-scatter.2.cloned.1.call-update) | async-done | bytes 1048592 | tf_op jit(solution)/shard_map/reduce_scatter | solution.py:115
  167.3 1.5 fusion.25
  168.8 1.6 fusion.24
  170.4 1.6 fusion.23
  172.0 1.6 fusion.22
  173.5 1.6 fusion.21
  175.1 1.5 fusion.20
  176.6 1.6 fusion.19
  178.2 1.6 fusion.18
  179.8 5.5 %all-to-all-start.1 = ((bf16[8,512,1,128]{1,3,2,0:T(8,128)(2,1)}), bf16[8,512,1,128]{1,3,2,0:T(8,128)(2,1)S(1)}, u32[]{:S(2)}, u32[]{:S(2)}) async-start(bf16[8,512,1,128]{1,3,2,0:T(8,128)(2,1)} %fusion.18), calls=%async_computation.2 | async-start | bytes 2097152 | tf_op jit(solution)/shard_map/all_to_all | solution.py:125
  185.3 0.1 reduce_sum.32
  185.4 0.1 copy.20
  185.5 0.0 copy-done.1
  185.5 0.2 copy.21
  185.7 0.0 copy-done.2
  185.7 0.1 copy.23
  185.9 25.1 %all-to-all-done.1 = bf16[8,512,1,128]{1,3,2,0:T(8,128)(2,1)S(1)} async-done(((bf16[8,512,1,128]{1,3,2,0:T(8,128)(2,1)}), bf16[8,512,1,128]{1,3,2,0:T(8,128)(2,1)S(1)}, u32[]{:S(2)}, u32[]{:S(2)}) %all-to-all-start.1) | async-done | bytes 1048608 | tf_op jit(solution)/shard_map/all_to_all | solution.py:125
  211.0 2.0 gather_fusion.1
  212.9 0.2 gather.15
  213.1 2.2 multiply_reduce_fusion
  215.4 0.8 fusion.17
  (21 shorter events, 0.3 us)
Async XLA Ops:
  6.5 21.1 %copy-start = (bf16[256,512]{1,0:T(8,128)(2,1)S(1)}, bf16[256,512]{1,0:T(8,128)(2,1)}, u32[]{:S(2)}) copy-start(bf16[256,512]{1,0:T(8,128)(2,1)} %param.14) | copy-start | bytes 786436
  6.5 96.7 %all-gather.3.cloned.1.call-start = ((), (), s32[]{:S(2)}) async-start(), calls=%async_computation.3 | async-start | bytes 5242880 | tf_op jit(solution)/shard_map/all_gather | solution.py:102
  7.4 12.7 %collective-permute-start = (bf16[15,64]{0,1:T(8,128)(2,1)S(1)}, bf16[15,64]{0,1:T(8,128)(2,1)S(1)}, u32[]{:S(2)}, u32[]{:S(2)}) collective-permute-start(bf16[15,64]{0,1:T(8,128)(2,1)S(1)} %slice.58), channel_id=1, source_target_pairs={{0,4},{4,8},{8,12},{12,16},{16,20},{20,24},{24,28},{1,5},{5,9},{9,... | collective-permute-start | bytes 5768 | tf_op jit(solution)/shard_map/ppermute | solution.py:18
  69.6 97.7 %reduce-scatter.2.cloned.1.call-start = ((), (), s32[]{:S(2)}) async-start(), calls=%async_computation.4 | async-start | bytes 5242880 | tf_op jit(solution)/shard_map/reduce_scatter | solution.py:115
  103.3 7.7 %copy-start.3 = (bf16[1,2048,1024]{2,1,0:T(8,128)(2,1)S(1)}, bf16[1,2048,1024]{2,1,0:T(8,128)(2,1)}, u32[]{:S(2)}) copy-start(bf16[1,2048,1024]{2,1,0:T(8,128)(2,1)} %param.20) | copy-start | bytes 12582916
  103.3 7.7 %copy-start.5 = (bf16[8,128,2048]{2,1,0:T(8,128)(2,1)S(1)}, bf16[8,128,2048]{2,1,0:T(8,128)(2,1)}, u32[]{:S(2)}) copy-start(bf16[8,128,2048]{2,1,0:T(8,128)(2,1)} %all-gather.3.cloned.1.call-done) | copy-start | bytes 12582916
  110.9 5.7 %copy-start.4 = (bf16[1,1024,2048]{2,1,0:T(8,128)(2,1)S(1)}, bf16[1,1024,2048]{2,1,0:T(8,128)(2,1)}, u32[]{:S(2)}) copy-start(bf16[1,1024,2048]{2,1,0:T(8,128)(2,1)} %param.21) | copy-start | bytes 12582916
  122.7 62.8 %copy-start.1 = (s32[256,2]{0,1:T(2,128)S(1)}, s32[256,2]{0,1:T(2,128)}, u32[]{:S(2)}) copy-start(s32[256,2]{0,1:T(2,128)} %param.17) | copy-start | bytes 6148
  122.7 63.0 %copy-start.2 = (f32[256,2]{0,1:T(2,128)S(1)}, f32[256,2]{0,1:T(2,128)}, u32[]{:S(2)}) copy-start(f32[256,2]{0,1:T(2,128)} %param.18) | copy-start | bytes 6148
  179.8 31.2 %all-to-all-start.1 = ((bf16[8,512,1,128]{1,3,2,0:T(8,128)(2,1)}), bf16[8,512,1,128]{1,3,2,0:T(8,128)(2,1)S(1)}, u32[]{:S(2)}, u32[]{:S(2)}) async-start(bf16[8,512,1,128]{1,3,2,0:T(8,128)(2,1)} %fusion.18), calls=%async_computation.2 | async-start | bytes 2097152 | tf_op jit(solution)/shard_map/all_to_all | solution.py:125
Sparse Core Ops, SparseCore 0:
  69.7 33.4 all-gather.2
  122.8 44.3 reduce-scatter.1
